TPU v7x, 256 devices: a 4x2x16 block of a 4x16x16 slice. The times are simulated.
256 devices in a mesh: grp: 2 (over y), ep: 64 (over z, x), tp: 2 (over core).
Axes of the slice: x: 4, y: 2, z: 16, core: 2. Of those that a mesh axis runs over, the one named last changes fastest.
The devices are a block of a 4x16x16 slice.
Arguments:
- fresh_inputs: bfloat16 [2048, 2048], P(('grp', 'ep')), parts along dimension 0, may hold values from -6 to 6
- memory_arrays: float32 [2048, 32, 64, 64], P(('grp', 'ep'), 'tp'), parts along dimension 0, may hold values from -4 to 4
- chosen_specialist: int32 [2048, 2], P(('grp', 'ep')), parts along dimension 0, may hold values from 0 to 3, all different within a row; in each aligned block of 1024 rows (0 to 1023, 1024 to 2047, ...) at most 768 rows name the same one
- chosen_coefficient: bfloat16 [2048, 2], P(('grp', 'ep')), parts along dimension 0, may hold values from 0.25 to 1
- first_rescale: float32 [2048], replicated, may hold values from 0.1 to 1.9
- second_rescale: float32 [2048], replicated, may hold values from 0.1 to 1.9
- receiver_projector: bfloat16 [2048, 2048], P('tp', 'ep'), may hold values from -0.125 to 0.125
- address_projector: bfloat16 [2048, 2048], P('tp', 'ep'), may hold values from -0.125 to 0.125
- content_projector: bfloat16 [2048, 2048], P('tp', 'ep'), may hold values from -0.125 to 0.125
- final_projector: bfloat16 [2048, 2048], P('tp', 'ep'), may hold values from -0.125 to 0.125
- forget_narrowing: bfloat16 [2048, 64], replicated, may hold values from -0.125 to 0.125
- forget_widening: bfloat16 [64, 2048], P(None, 'tp'), may hold values from -0.75 to 0.75
- forget_bias: float32 [2048], P('tp'), may hold values from -3 to 1
- learning_narrowing: bfloat16 [2048, 64], replicated, may hold values from -0.125 to 0.125
- learning_widening: bfloat16 [64, 2048], P(None, 'tp'), may hold values from -0.75 to 0.75
- learning_bias: float32 [2048], P('tp'), may hold values from -1.5 to 1.5
- lane_scaling: float32 [2048], P('tp'), may hold values from 0.1 to 1.9
- instant_reward: float32 [32, 64], P('tp'), may hold values from -0.5 to 0.5
- specialist_switch: bfloat16 [2048, 28672], P(None, ('ep', 'tp')), may hold values from -0.125 to 0.125
- specialist_expand: bfloat16 [2048, 28672], P(None, ('ep', 'tp')), may hold values from -0.125 to 0.125
- specialist_contract: bfloat16 [28672, 2048], P(('ep', 'tp')), may hold values from -0.0625 to 0.0625
- common_activator: bfloat16 [2048, 5632], P(None, ('ep', 'tp')), may hold values from -0.125 to 0.125
- common_expand: bfloat16 [2048, 5632], P(None, ('ep', 'tp')), may hold values from -0.125 to 0.125
- common_contract: bfloat16 [5632, 2048], P(('ep', 'tp')), may hold values from -0.078125 to 0.078125
- common_switch: bfloat16 [2048], replicated, may hold values from -0.125 to 0.125
Outputs:
- new_tokens: bfloat16 [2048, 2048], P(('grp', 'ep', 'tp')), parts along dimension 0
- memory_after: float32 [2048, 32, 64, 64], P(('grp', 'ep'), 'tp'), parts along dimension 0
There are 2 independent parts, one for each index of `grp`. A program takes and returns all parts, laid end to end along the dimension named above; an argument that names none is the same for every part. Nothing has to cross between parts.
Inputs may be any that keep to these rules, and one draw needn't show every extreme that they name: `chosen_specialist`: each row names 2 different experts. Over the whole batch no expert is named by more than 768 rows, and in every draw some expert is named by exactly 768 rows.
All inputs are finite; a program needn't handle non-finite values.
Results may differ from a plain program's by a relative error of at most 0.014.
Values may be sent and summed in bfloat16 or wider, within the bound.
No kernel may reach another device: no remote copies, remote signals or barrier semaphores. Data moves between devices by JAX's collectives and lax.ppermute only.
A program may use at most 128 MiB of HBM per device.

v0:
```python
import jax
import jax.numpy as jnp
from jax import lax
from jax.sharding import Mesh
from jax.sharding import PartitionSpec as P

LANE_WIDTH = 64
FF_E = 7168
EP = ("ep_0", "ep_1")
GRP_EP = ("grp", "ep_0", "ep_1")
EP_TP = ("ep_0", "ep_1", "tp")
GRP_EP_TP = ("grp", "ep_0", "ep_1", "tp")
RMS_EPS = 1e-06
GROUP_EPS = 0.00064
HIGHEST = lax.Precision.HIGHEST


def turned_gather(arrays, axis, dims):
    turned = [jnp.moveaxis(a, dim, 0) for a, dim in zip(arrays, dims)]
    widths = [t[0].size for t in turned]
    both = jnp.concatenate([t.reshape(-1, w) for t, w in zip(turned, widths)], axis=1)
    whole = lax.all_gather(both, axis, axis=0, tiled=True)
    blocks = jnp.split(whole, [sum(widths[:k]) for k in range(1, len(widths))], axis=1)
    return tuple(
        (
            jnp.moveaxis(b.reshape(-1, *t.shape[1:]), 0, dim)
            for b, t, dim in zip(blocks, turned, dims)
        )
    )


def from_everyone(value, axis):
    copies = jnp.broadcast_to(value, (lax.axis_size(axis), *value.shape))
    return lax.all_to_all(copies, axis, split_axis=0, concat_axis=0, tiled=True)


def of_everyone(value, axis):
    return from_everyone(value, axis).astype(jnp.float32).sum(axis=0)


def whole_of(value, axes, dim):
    if not axes:
        return value
    nearer = lax.all_gather(value, axes[-1], axis=dim, tiled=True)
    return whole_of(nearer, axes[:-1], dim)


def side_by_side(arrays, axis, dim, along):
    ends, at = ([], 0)
    for a in arrays[:-1]:
        at += a.shape[along]
        ends.append(at)
    both = jnp.concatenate(arrays, axis=along)
    return tuple(jnp.split(lax.all_gather(both, axis, axis=dim, tiled=True), ends, axis=along))


def in_order(blocks, dim):
    dims = list(blocks.shape[1:])
    dims[dim] *= blocks.shape[0]
    return jnp.moveaxis(blocks, 0, dim).reshape(dims)


def one_gather(arrays, axis, dims):
    ravelled = jnp.concatenate([a.reshape(-1) for a in arrays])
    lines, at, finished = (lax.all_gather(ravelled, axis), 0, [])
    for a, dim in zip(arrays, dims):
        blocks = lines[:, at : at + a.size].reshape(-1, *a.shape)
        finished.append(in_order(blocks, dim))
        at += a.size
    return tuple(finished)


def cut_along(value, dim, devices):
    dims = value.shape
    blocks = value.reshape(*dims[:dim], devices, dims[dim] // devices, *dims[dim + 1 :])
    return jnp.moveaxis(blocks, dim, 0)


def sent_and_summed(value, axis, dim):
    devices = lax.axis_size(axis)
    blocks = lax.all_to_all(cut_along(value, dim, devices), axis, 0, 0, tiled=True)
    return jnp.sum(blocks.astype(jnp.float32), axis=0)


def rms_norm(values, norm_gain):
    mean_sq = jnp.mean(values * values, axis=-1, keepdims=True)
    return values * lax.rsqrt(mean_sq + RMS_EPS) * norm_gain


def widen(rounded):
    return lax.optimization_barrier(rounded).astype(jnp.float32)


def evolve_memory(
    memory_arrays,
    receiver_lanes,
    address_lanes,
    content_lanes,
    forget_lanes,
    learning_lanes,
    lane_rescale,
    instant_reward,
):
    unit_key = address_lanes * lax.rsqrt(
        jnp.sum(address_lanes * address_lanes, axis=-1, keepdims=True) + 1.0
    )
    stepped_address = address_lanes * learning_lanes
    removal = jnp.einsum("bhvk,bhk->bhv", memory_arrays, unit_key, precision=HIGHEST)
    memory_after = (
        memory_arrays * forget_lanes[:, :, None, :]
        - removal[..., None] * (unit_key * learning_lanes)[:, :, None, :]
        + content_lanes[..., None] * stepped_address[:, :, None, :]
    )
    memory_retrieval = jnp.einsum("bhvk,bhk->bhv", memory_after, receiver_lanes, precision=HIGHEST)
    centred = memory_retrieval - jnp.mean(memory_retrieval, axis=-1, keepdims=True)
    unit_address = centred * lax.rsqrt(
        jnp.mean(centred * centred, axis=-1, keepdims=True) + GROUP_EPS
    )
    instant_extra = (
        jnp.sum(receiver_lanes * stepped_address * instant_reward, axis=-1, keepdims=True)
        * content_lanes
    )
    return (memory_after, unit_address * lane_rescale + instant_extra)


def swiglu(rows_in, gate_w, up_w):
    gate_val = jnp.dot(rows_in, gate_w, preferred_element_type=jnp.float32)
    up_val = jnp.dot(rows_in, up_w, preferred_element_type=jnp.float32)
    return (jax.nn.silu(gate_val) * up_val).astype(jnp.bfloat16)


def body(
    fresh_inputs,
    memory_arrays,
    chosen_specialist,
    chosen_coefficient,
    first_rescale,
    second_rescale,
    receiver_projector,
    address_projector,
    content_projector,
    final_projector,
    forget_narrowing,
    forget_widening,
    forget_bias,
    learning_narrowing,
    learning_widening,
    learning_bias,
    lane_scaling,
    instant_reward,
    specialist_switch,
    specialist_expand,
    specialist_contract,
    common_activator,
    common_expand,
    common_contract,
    common_switch,
):
    own_rows = fresh_inputs.shape[0]
    model_width = fresh_inputs.shape[1]
    tp_count = lax.axis_size("tp")
    tp_rank = lax.axis_index("tp")
    half_width = model_width // tp_count
    head_count = half_width // LANE_WIDTH
    residual = fresh_inputs.astype(jnp.float32)
    normed = rms_norm(residual, first_rescale).astype(jnp.bfloat16)
    normed_half = lax.dynamic_slice_in_dim(normed, tp_rank * half_width, half_width, 1)
    pieces = turned_gather(
        (receiver_projector, address_projector, content_projector), EP, (1, 1, 1)
    )
    partials = tuple(
        (
            jnp.dot(normed_half, weight_block, preferred_element_type=jnp.float32)
            for weight_block in pieces
        )
    )
    partial_value = jnp.stack(partials, axis=1).astype(jnp.bfloat16)
    projected = (
        of_everyone(widen(partial_value).astype(jnp.bfloat16), "tp")
        .astype(jnp.float32)
        .astype(jnp.bfloat16)
    )
    mine = lax.dynamic_slice_in_dim(projected, tp_rank * half_width, half_width, 2)

    def divide_lanes(channels):
        return channels.astype(jnp.float32).reshape(own_rows, head_count, LANE_WIDTH)

    decay_mid = jnp.tanh(
        jnp.dot(normed, forget_narrowing, preferred_element_type=jnp.float32)
    ).astype(jnp.bfloat16)
    decay_pre = forget_bias + jnp.dot(
        decay_mid, forget_widening, preferred_element_type=jnp.float32
    )
    decay_vals = jnp.exp(-jnp.exp(-jax.nn.softplus(-decay_pre) - 0.5))
    rate_mid = jnp.dot(normed, learning_narrowing, preferred_element_type=jnp.float32).astype(
        jnp.bfloat16
    )
    rate_vals = jax.nn.sigmoid(
        learning_bias + jnp.dot(rate_mid, learning_widening, preferred_element_type=jnp.float32)
    )
    memory_after, memory_retrieval = evolve_memory(
        memory_arrays,
        divide_lanes(mine[:, 0]),
        divide_lanes(mine[:, 1]),
        divide_lanes(mine[:, 2]),
        divide_lanes(decay_vals),
        divide_lanes(rate_vals),
        lane_scaling.reshape(head_count, LANE_WIDTH),
        instant_reward,
    )
    attended = memory_retrieval.reshape(own_rows, half_width).astype(jnp.bfloat16)
    out_part = jnp.dot(
        attended, whole_of(final_projector, EP, 1), preferred_element_type=jnp.float32
    ).astype(jnp.bfloat16)
    mixed_out = (
        of_everyone(widen(out_part).astype(jnp.bfloat16), "tp")
        .astype(jnp.float32)
        .astype(jnp.bfloat16)
    )
    residual = residual + mixed_out.astype(jnp.float32)
    ffn_in = rms_norm(residual, second_rescale).astype(jnp.bfloat16)
    all_in, all_weight, all_ids = (
        *side_by_side((ffn_in, chosen_coefficient), EP, 0, 1),
        lax.all_gather(chosen_specialist, EP, axis=0, tiled=True),
    )
    column_count = specialist_switch.shape[1]
    flat_rank = lax.axis_index(EP) * tp_count + tp_rank
    expert = flat_rank * column_count // FF_E
    expert_share = jnp.sum(
        jnp.where(all_ids == expert, all_weight.astype(jnp.float32), 0.0), axis=1
    )
    hidden = swiglu(all_in, specialist_switch, specialist_expand)
    shared_hidden = swiglu(all_in, common_activator, common_expand)
    branch_scale = jax.nn.sigmoid(
        jnp.dot(all_in, common_switch, preferred_element_type=jnp.float32)
    )
    rows_mine = own_rows // tp_count
    hidden_pair, shared_pair = one_gather((hidden, shared_hidden), "tp", (1, 1))
    down_half, shared_half = (
        lax.all_to_all(specialist_contract, "tp", split_axis=1, concat_axis=0, tiled=True),
        lax.all_to_all(common_contract, "tp", split_axis=1, concat_axis=0, tiled=True),
    )
    half_total = expert_share[:, None] * jnp.dot(
        hidden_pair, down_half, preferred_element_type=jnp.float32
    )
    half_total = half_total + branch_scale[:, None] * jnp.dot(
        shared_pair, shared_half, preferred_element_type=jnp.float32
    )
    half_rows = sent_and_summed(half_total.astype(jnp.bfloat16), EP, 0)
    routed = lax.all_to_all(half_rows, "tp", split_axis=0, concat_axis=1, tiled=True)
    own_residual = lax.dynamic_slice_in_dim(residual, tp_rank * rows_mine, rows_mine, 0)
    return ((own_residual + routed).astype(jnp.bfloat16), memory_after)


def solution(mesh):
    torus = Mesh(
        mesh.devices.reshape(mesh.shape["grp"], 16, 4, mesh.shape["tp"]),
        ("grp", "ep_0", "ep_1", "tp"),
    )
    return jax.shard_map(
        body,
        mesh=torus,
        in_specs=(
            P(GRP_EP, None),
            P(GRP_EP, "tp", None, None),
            P(GRP_EP, None),
            P(GRP_EP, None),
            P(),
            P(),
            P("tp", EP),
            P("tp", EP),
            P("tp", EP),
            P("tp", EP),
            P(),
            P(None, "tp"),
            P("tp"),
            P(),
            P(None, "tp"),
            P("tp"),
            P("tp"),
            P("tp", None),
            P(None, EP_TP),
            P(None, EP_TP),
            P(EP_TP, None),
            P(None, EP_TP),
            P(None, EP_TP),
            P(EP_TP, None),
            P(),
        ),
        out_specs=(P(GRP_EP_TP, None), P(GRP_EP, "tp", None, None)),
        check_vma=False,
    )
```

profile of v0, /device:TPU:33, one launch (start us, length us, event | category | flops | bytes accessed | tf_op | source)
XLA Modules:
  0.0 657.6 jit_solution(10418199914732399732)
XLA Ops:
  7.3 1.7 pad_maximum_fusion.1
  9.1 12.9 %all_gather.22 = bf16[1024,128]{0,1:T(8,128)(2,1)} all-gather(bf16[1024,32]{0,1:T(8,128)(2,1)} %param.34), channel_id=1, replica_groups=mesh['grp'=2,'ep_0'=16,'ep_1'=4,'tp'=2] {'ep_1'}, dimensions={1}, use_global_device_ids=true | all-gather | bytes 327680 | tf_op jit(solution)/shard_map/all_gather | solution.py:44
  25.5 1.4 fusion.55
  26.9 1.4 fusion.71
  28.5 161.8 %all-gather.7.cloned.1.call-done = bf16[2048,3072]{1,0:T(8,128)(2,1)} async-done(((bf16[32,3072]{1,0:T(8,128)(2,1)}), bf16[2048,3072]{1,0:T(8,128)(2,1)}) %all-gather.7.cloned.1.call-update) | async-done | bytes 12582928 | tf_op jit(solution)/shard_map/all_gather | solution.py:22
  190.3 3.4 fusion.18
  193.6 3.5 fusion.21
  197.1 3.4 fusion.24
  200.6 6.9 %all_to_all.66 = bf16[2,16,3,2048]{3,1,2,0:T(8,128)(2,1)S(1)} all-to-all(bf16[2,16,3,2048]{3,1,2,0:T(8,128)(2,1)S(1)} %broadcast_in_dim.7), channel_id=1, replica_groups=mesh['grp'=2,'ep_0'=16,'ep_1'=4,'tp'=2] {'tp'}, dimensions={0} | all-to-all | bytes 786432 | tf_op jit(solution)/shard_map/all_to_all | solution.py:34
  208.2 15.4 %fusion.80 = f32[16,16,1,64]{3,2,1,0:T(1,128)S(1)} fusion(f32[16,16,64,1]{2,3,1,0:T(1,128)S(1)} %bitcast.83, f32[16,16,64,64]{3,2,1,0:T(8,128)} %param.26), kind=kOutput, calls=%fused_computation.96 | convolution fusion | flops 12582912 | bytes 4325376 | tf_op jit(solution)/shard_map/bhvk,bhk->bhv/dot_general | solution.py:108
  223.6 8.8 %multiply_add_fusion = f32[16,16,64,64]{3,2,1,0:T(8,128)S(1)} fusion(f32[16,16,64,64]{3,2,1,0:T(8,128)} %param.26, f32[16,16,64]{2,1,0:T(8,128)S(1)} %get-tuple-element.8, f32[16,16,64]{2,1,0:T(8,128)S(1)} %reshape.133, f32[16,16,64]{2,1,0:T(8,128)S(1)} %get-tuple-element.6, f32[16,16,64]{2,1,0:T(8,128)S(1)} %bitcast.82, f32[16,16,64]{2,1,0:T(8,128)S(1)} %mul.210), kind=kLoop, calls=%fused_computation.1 | loop fusion | flops 5242880 | bytes 8716288 | tf_op jit(solution)/shard_map/add | solution.py:110
  232.4 6.6 %fusion.81 = f32[16,16,1,64]{3,2,1,0:T(1,128)S(1)} fusion(f32[16,16,64,64]{3,2,1,0:T(8,128)S(1)} %multiply_add_fusion, bf16[16,16,64,1]{2,3,1,0:T(2,128)(2,1)S(1)} %reshape.148), kind=kOutput, calls=%fused_computation.97 | convolution fusion | flops 12582912 | bytes 4292608 | tf_op jit(solution)/shard_map/bhvk,bhk->bhv/dot_general | solution.py:114
  240.0 16.9 %all-gather.9.cloned.1.call-done = bf16[1024,2048]{0,1:T(8,128)(2,1)} async-done(((bf16[1024,128]{0,1:T(8,128)(2,1)}), bf16[1024,2048]{0,1:T(8,128)(2,1)}) %all-gather.9.cloned.1.call-update) | async-done | bytes 4194320 | tf_op jit(solution)/shard_map/all_gather | solution.py:44
  257.0 3.4 convolution_convert_fusion
  260.4 13.1 %all_to_all.67 = bf16[2,16,2048]{2,1,0:T(8,128)(2,1)S(1)} all-to-all(bf16[2,16,2048]{2,1,0:T(8,128)(2,1)S(1)} %broadcast_in_dim.8), channel_id=1, replica_groups=mesh['grp'=2,'ep_0'=16,'ep_1'=4,'tp'=2] {'tp'}, dimensions={0} | all-to-all | bytes 262144 | tf_op jit(solution)/shard_map/all_to_all | solution.py:34
  274.8 129.9 %all-gather.11.cloned.1.call-done = bf16[1024,2050]{1,0:T(8,128)(2,1)} async-done(((bf16[16,2050]{1,0:T(8,128)(2,1)}), bf16[1024,2050]{1,0:T(8,128)(2,1)}) %all-gather.11.cloned.1.call-update) | async-done | bytes 4198416 | tf_op jit(solution)/shard_map/all_gather | solution.py:54
  404.7 3.7 fusion.31
  408.5 1.3 fusion.46
  410.5 3.7 fusion.35
  414.3 1.4 fusion.40
  419.0 13.5 %all-to-all-start.2 = ((bf16[224,2,1024]{2,0,1:T(8,128)(2,1)}), bf16[224,2,1024]{2,0,1:T(8,128)(2,1)S(1)}, u32[]{:S(2)}, u32[]{:S(2)}) async-start(bf16[224,2,1024]{2,0,1:T(8,128)(2,1)} %bitcast.75), calls=%async_computation.2 | async-start | bytes 1835008 | tf_op jit(solution)/shard_map/all_to_all | solution.py:240
  432.5 61.6 %all-gather.1 = s32[64,16,2]{1,2,0:T(2,128)S(1)} all-gather(s32[1,16,2]{1,2,0:T(2,128)S(1)} %bitcast.90), channel_id=1, replica_groups=mesh['grp'=2,'ep_0'=16,'ep_1'=4,'tp'=2] {'ep_0','ep_1'}, dimensions={0}, use_global_device_ids=true | all-gather | bytes 8320 | tf_op jit(solution)/shard_map/all_gather | solution.py:224
  495.4 3.4 fusion.27
  498.8 1.5 reshape.134
  501.2 1.4 reshape.129
  503.9 1.5 reshape.130
  505.7 22.6 %all-to-all-start.3 = ((bf16[44,2,1024]{2,0,1:T(8,128)(2,1)}), bf16[44,2,1024]{2,0,1:T(8,128)(2,1)S(1)}, u32[]{:S(2)}, u32[]{:S(2)}) async-start(bf16[44,2,1024]{2,0,1:T(8,128)(2,1)} %copy.77), calls=%async_computation.3 | async-start | bytes 393216 | tf_op jit(solution)/shard_map/all_to_all | solution.py:241
  528.2 4.4 fusion.58
  532.7 4.4 fusion.8
  537.0 9.9 %all-to-all-start.4 = ((bf16[64,16,1024]{2,1,0:T(8,128)(2,1)}), bf16[64,16,1024]{2,1,0:T(8,128)(2,1)S(1)}, u32[]{:S(2)}, u32[]{:S(2)}) async-start(bf16[64,16,1024]{2,1,0:T(8,128)(2,1)} %bitcast.20), calls=%async_computation.4 | async-start | bytes 4194304 | tf_op jit(solution)/shard_map/all_to_all | solution.py:81
  546.9 95.3 %all-to-all-done.4 = bf16[64,16,1024]{2,1,0:T(8,128)(2,1)S(1)} async-done(((bf16[64,16,1024]{2,1,0:T(8,128)(2,1)}), bf16[64,16,1024]{2,1,0:T(8,128)(2,1)S(1)}, u32[]{:S(2)}, u32[]{:S(2)}) %all-to-all-start.4) | async-done | bytes 2097184 | tf_op jit(solution)/shard_map/all_to_all | solution.py:81
  642.6 7.9 %all_to_all.68 = f32[2,8,1024]{2,1,0:T(8,128)S(1)} all-to-all(f32[2,8,1024]{2,1,0:T(8,128)S(1)} %bitcast.84), channel_id=1, replica_groups=mesh['grp'=2,'ep_0'=16,'ep_1'=4,'tp'=2] {'tp'}, dimensions={0} | all-to-all | bytes 131072 | tf_op jit(solution)/shard_map/all_to_all | solution.py:250
  (98 shorter events, 15.4 us)
Async XLA Ops:
  7.2 403.3 %copy-start = (bf16[2048,224]{0,1:T(8,128)(2,1)S(1)}, bf16[2048,224]{0,1:T(8,128)(2,1)}, u32[]{:S(2)}) copy-start(bf16[2048,224]{0,1:T(8,128)(2,1)} %param.43) | copy-start | bytes 2752516
  7.2 183.1 %all-gather.7.cloned.1.call-start = ((), (), s32[]{:S(2)}) async-start(), calls=%async_computation.6 | async-start | bytes 12779520 | tf_op jit(solution)/shard_map/all_gather | solution.py:22
  9.0 248.0 %all-gather.9.cloned.1.call-start = ((), (), s32[]{:S(2)}) async-start(), calls=%async_computation.7 | async-start | bytes 4456448 | tf_op jit(solution)/shard_map/all_gather | solution.py:44
  22.0 382.7 %all-gather.11.cloned.1.call-start = ((), (), s32[]{:S(2)}) async-start(), calls=%async_computation.8 | async-start | bytes 4526080 | tf_op jit(solution)/shard_map/all_gather | solution.py:54
  232.4 6.6 %copy-start.2 = (f32[16,16,64,64]{3,2,1,0:T(8,128)}, f32[16,16,64,64]{3,2,1,0:T(8,128)S(1)}, u32[]{:S(2)}) copy-start(f32[16,16,64,64]{3,2,1,0:T(8,128)S(1)} %multiply_add_fusion) | copy-start | bytes 12582916
  232.4 7.0 %copy-start.7 = (f32[16,64]{1,0:T(8,128)S(1)}, f32[16,64]{1,0:T(8,128)}, u32[]{:S(2)}) copy-start(f32[16,64]{1,0:T(8,128)} %param.42) | copy-start | bytes 12292
  239.0 34.5 %copy-start.4 = (bf16[16,2048]{1,0:T(8,128)(2,1)S(1)}, bf16[16,2048]{1,0:T(8,128)(2,1)}, u32[]{:S(2)}) copy-start(bf16[16,2048]{1,0:T(8,128)(2,1)} %param.25) | copy-start | bytes 196612
  239.0 34.7 %copy-start.8 = (f32[2048]{0:T(1024)S(1)}, f32[2048]{0:T(1024)}, u32[]{:S(2)}) copy-start(f32[2048]{0:T(1024)} %param.30) | copy-start | bytes 24580
  239.0 165.7 %copy-start.12 = (bf16[2048,44]{0,1:T(8,128)(2,1)S(1)}, bf16[2048,44]{0,1:T(8,128)(2,1)}, u32[]{:S(2)}) copy-start(bf16[2048,44]{0,1:T(8,128)(2,1)} %param.46) | copy-start | bytes 540676
  274.5 134.0 %copy-start.13 = (bf16[2048,44]{0,1:T(8,128)(2,1)S(1)}, bf16[2048,44]{0,1:T(8,128)(2,1)}, u32[]{:S(2)}) copy-start(bf16[2048,44]{0,1:T(8,128)(2,1)} %param.47) | copy-start | bytes 540676
  274.5 224.3 %all-gather.13.cloned.1.call-start = ((), (), s32[]{:S(2)}) async-start(), calls=%async_computation.9 | async-start | bytes 1646592 | tf_op jit(solution)/shard_map/all_gather | solution.py:65
  404.7 3.7 copy-start.3
  410.0 4.3 slice-start
  410.5 3.8 slice-start.1
  410.5 3.8 copy-start.11
  415.8 2.2 copy-start.5
  415.8 16.7 %copy-start.9 = (bf16[2048]{0:T(1024)(128)(2,1)S(1)}, bf16[2048]{0:T(1024)(128)(2,1)}, u32[]{:S(2)}) copy-start(bf16[2048]{0:T(1024)(128)(2,1)} %param.49) | copy-start | bytes 12292
  415.8 16.7 %copy-start.10 = (s32[16,2]{0,1:T(2,128)S(1)}, s32[16,2]{0,1:T(2,128)}, u32[]{:S(2)}) copy-start(s32[16,2]{0,1:T(2,128)} %param.27) | copy-start | bytes 388
  415.8 78.6 %copy-start.6 = (bf16[44,2048]{1,0:T(8,128)(2,1)S(1)}, bf16[44,2048]{1,0:T(8,128)(2,1)}, u32[]{:S(2)}) copy-start(bf16[44,2048]{1,0:T(8,128)(2,1)} %param.48) | copy-start | bytes 540676
  415.8 79.4 %slice-start.2 = ((bf16[1024,2050]{1,0:T(8,128)(2,1)}), bf16[1024,2]{1,0:T(8,128)(2,1)S(1)}, s32[]{:S(2)}) async-start(bf16[1024,2050]{1,0:T(8,128)(2,1)} %all-gather.11.cloned.1.call-done), calls=%async_computation.12 | async-start | bytes 524288 | tf_op jit(solution)/shard_map/split | solution.py:54
  419.0 86.7 %all-to-all-start.2 = ((bf16[224,2,1024]{2,0,1:T(8,128)(2,1)}), bf16[224,2,1024]{2,0,1:T(8,128)(2,1)S(1)}, u32[]{:S(2)}, u32[]{:S(2)}) async-start(bf16[224,2,1024]{2,0,1:T(8,128)(2,1)} %bitcast.75), calls=%async_computation.2 | async-start | bytes 1835008 | tf_op jit(solution)/shard_map/all_to_all | solution.py:240
  505.7 27.0 %all-to-all-start.3 = ((bf16[44,2,1024]{2,0,1:T(8,128)(2,1)}), bf16[44,2,1024]{2,0,1:T(8,128)(2,1)S(1)}, u32[]{:S(2)}, u32[]{:S(2)}) async-start(bf16[44,2,1024]{2,0,1:T(8,128)(2,1)} %copy.77), calls=%async_computation.3 | async-start | bytes 393216 | tf_op jit(solution)/shard_map/all_to_all | solution.py:241
  532.7 118.5 %copy-start.1 = (bf16[2048,224]{0,1:T(8,128)(2,1)S(1)}, bf16[2048,224]{0,1:T(8,128)(2,1)}, u32[]{:S(2)}) copy-start(bf16[2048,224]{0,1:T(8,128)(2,1)} %param.43) | copy-start | bytes 2752516
  537.0 105.3 %all-to-all-start.4 = ((bf16[64,16,1024]{2,1,0:T(8,128)(2,1)}), bf16[64,16,1024]{2,1,0:T(8,128)(2,1)S(1)}, u32[]{:S(2)}, u32[]{:S(2)}) async-start(bf16[64,16,1024]{2,1,0:T(8,128)(2,1)} %bitcast.20), calls=%async_computation.4 | async-start | bytes 4194304 | tf_op jit(solution)/shard_map/all_to_all | solution.py:81
Sparse Core Ops, SparseCore 0:
  11.0 179.2 all-gather.6
  192.1 64.8 all-gather.8
  274.6 130.0 all-gather.10
  418.1 23.4 all-gather.12
where the time goes:
time: 659 us; the launch traced here: 658 us
  waiting for transfers between devices  404 us (61%)
  blocking collectives  102 us (15%)
  matrix products  60.8 us (9%)
  starting transfers between devices  46.5 us (7%)
  other arithmetic  16.3 us (2%)
  between operations  14.3 us (2%)
  local copies, waits for them, and re-layouts  13.2 us (2%)
    all_gather x1, waiting for transfers between devices, turned_gather(): whole = lax.all_gather(both, axis, axis=0, tiled=True)  162 us
    all_gather x1, waiting for transfers between devices, side_by_side(): lax.all_gather(both, axis, axis=dim, tiled=True)  130 us
    all_to_all x1, waiting for transfers between devices, sent_and_summed(): lax.all_to_all(cut_along(value, dim, devices), axis, 0, 0, tiled=True)  95.3 us
    all_gather x1, blocking collectives, body(): lax.all_gather(chosen_specialist, EP, axis=0, tiled=True)  61.6 us
    all_to_all x1, starting transfers between devices, body(): lax.all_to_all(common_contract, 'tp', split_axis=1, concat_axis=0, tiled=...  22.6 us
    all_to_all x2, blocking collectives, from_everyone(): return lax.all_to_all(copies, axis, split_axis=0, concat_axis=0, tiled=True)  20 us
    all_gather x1, waiting for transfers between devices, whole_of(): nearer = lax.all_gather(value, axes[-1], axis=dim, tiled=True)  16.9 us
    dot_general x1, matrix products, evolve_memory(): jnp.einsum('bhvk,bhk->bhv', memory_arrays, unit_key, precision=HIGHEST)  15.4 us
  transfers between devices with their start and end apart: 7, of which 4 were waited for; matrix products, arithmetic and copies ran while one was open for 10% of the time, Pallas kernels for 0%

commit v1 on v0

--- a/solution.py
+++ b/solution.py
@@ -13,6 +13,13 @@
 RMS_EPS = 1e-06
 GROUP_EPS = 0.00064
 HIGHEST = lax.Precision.HIGHEST
+
+
+def all_by_exchange(array, name, along):
+    size = lax.axis_size(name)
+    blocks = jnp.stack([array for _ in range(size)])
+    blocks = lax.all_to_all(blocks, name, split_axis=0, concat_axis=0)
+    return jnp.concatenate(blocks, axis=along)
 
 
 def turned_gather(arrays, axis, dims):
@@ -221,7 +228,7 @@
     ffn_in = rms_norm(residual, second_rescale).astype(jnp.bfloat16)
     all_in, all_weight, all_ids = (
         *side_by_side((ffn_in, chosen_coefficient), EP, 0, 1),
-        lax.all_gather(chosen_specialist, EP, axis=0, tiled=True),
+        all_by_exchange(chosen_specialist, EP, 0),
     )
     column_count = specialist_switch.shape[1]
     flat_rank = lax.axis_index(EP) * tp_count + tp_rank

time: 659 us -> 599 us (0.909)
  blocking collectives: 102 us -> 39.7 us
  waiting for transfers between devices: 404 us -> 416 us
  starting transfers between devices: 46.5 us -> 36.3 us
    all_gather x1 -> x0, blocking collectives: 61.6 us -> none  [body(): lax.all_gather(chosen_specialist, EP, axis=0, tiled=True)]
    all_to_all x1, starting transfers between devices: 22.6 us -> 3.73 us  [body(): lax.all_to_all(common_contract, 'tp', split_axis=1, concat_axis=0, tiled=...]
    all_to_all x0 -> x1, waiting for transfers between devices: none -> 10.9 us  [all_by_exchange(): blocks = lax.all_to_all(blocks, name, split_axis=0, concat_axis=0)]
    all_to_all x0 -> x1, starting transfers between devices: none -> 10.4 us  [all_by_exchange(): blocks = lax.all_to_all(blocks, name, split_axis=0, concat_axis=0)]
  transfers between devices with their start and end apart: 7 -> 8, of which waited for: 4 -> 5; matrix products, arithmetic and copies ran while one was open for 10% -> 11% of each run, Pallas kernels for 0% -> 0%
where the time goes in v1:
time: 599 us; the launch traced here: 597 us
  waiting for transfers between devices  416 us (69%)
  matrix products  60.8 us (10%)
  blocking collectives  39.7 us (7%)
  starting transfers between devices  36.3 us (6%)
  other arithmetic  16.3 us (3%)
  between operations  14.3 us (2%)
  local copies, waits for them, and re-layouts  13.8 us (2%)
    all_gather x1, waiting for transfers between devices, turned_gather(): whole = lax.all_gather(both, axis, axis=0, tiled=True)  162 us
    all_gather x1, waiting for transfers between devices, side_by_side(): lax.all_gather(both, axis, axis=dim, tiled=True)  130 us
    all_to_all x1, waiting for transfers between devices, sent_and_summed(): lax.all_to_all(cut_along(value, dim, devices), axis, 0, 0, tiled=True)  96.3 us
    all_to_all x2, blocking collectives, from_everyone(): return lax.all_to_all(copies, axis, split_axis=0, concat_axis=0, tiled=True)  20 us
    all_gather x1, waiting for transfers between devices, whole_of(): nearer = lax.all_gather(value, axes[-1], axis=dim, tiled=True)  16.9 us
    dot_general x1, matrix products, evolve_memory(): jnp.einsum('bhvk,bhk->bhv', memory_arrays, unit_key, precision=HIGHEST)  15.4 us
    all_to_all x1, starting transfers between devices, body(): lax.all_to_all(specialist_contract, 'tp', split_axis=1, concat_axis=0, ti...  15.2 us
    all_gather x1, blocking collectives, whole_of(): nearer = lax.all_gather(value, axes[-1], axis=dim, tiled=True)  12.9 us
  transfers between devices with their start and end apart: 8, of which 5 were waited for; matrix products, arithmetic and copies ran while one was open for 11% of the time, Pallas kernels for 0%

profile of v1, /device:TPU:33, one launch (start us, length us, event | category | flops | bytes accessed | tf_op | source)
XLA Modules:
  0.0 597.4 jit_solution(15757787576377323111)
XLA Ops:
  7.3 1.7 pad_maximum_fusion.1
  9.1 12.9 %all_gather.19 = bf16[1024,128]{0,1:T(8,128)(2,1)} all-gather(bf16[1024,32]{0,1:T(8,128)(2,1)} %param.34), channel_id=1, replica_groups=mesh['grp'=2,'ep_0'=16,'ep_1'=4,'tp'=2] {'ep_1'}, dimensions={1}, use_global_device_ids=true | all-gather | bytes 327680 | tf_op jit(solution)/shard_map/all_gather | solution.py:51
  25.5 1.4 fusion.55
  27.0 1.4 fusion.71
  28.5 161.8 %all-gather.6.cloned.1.call-done = bf16[2048,3072]{1,0:T(8,128)(2,1)} async-done(((bf16[32,3072]{1,0:T(8,128)(2,1)}), bf16[2048,3072]{1,0:T(8,128)(2,1)}) %all-gather.6.cloned.1.call-update) | async-done | bytes 12582928 | tf_op jit(solution)/shard_map/all_gather | solution.py:29
  190.3 3.4 fusion.18
  193.7 3.4 fusion.21
  197.1 3.4 fusion.24
  200.5 6.9 %all_to_all.71 = bf16[2,16,3,2048]{3,1,2,0:T(8,128)(2,1)S(1)} all-to-all(bf16[2,16,3,2048]{3,1,2,0:T(8,128)(2,1)S(1)} %broadcast_in_dim.7), channel_id=1, replica_groups=mesh['grp'=2,'ep_0'=16,'ep_1'=4,'tp'=2] {'tp'}, dimensions={0} | all-to-all | bytes 786432 | tf_op jit(solution)/shard_map/all_to_all | solution.py:41
  208.2 15.4 %fusion.80 = f32[16,16,1,64]{3,2,1,0:T(1,128)S(1)} fusion(f32[16,16,64,1]{2,3,1,0:T(1,128)S(1)} %bitcast.82, f32[16,16,64,64]{3,2,1,0:T(8,128)} %param.26), kind=kOutput, calls=%fused_computation.96 | convolution fusion | flops 12582912 | bytes 4325376 | tf_op jit(solution)/shard_map/bhvk,bhk->bhv/dot_general | solution.py:115
  223.6 8.8 %multiply_add_fusion = f32[16,16,64,64]{3,2,1,0:T(8,128)S(1)} fusion(f32[16,16,64,64]{3,2,1,0:T(8,128)} %param.26, f32[16,16,64]{2,1,0:T(8,128)S(1)} %get-tuple-element.8, f32[16,16,64]{2,1,0:T(8,128)S(1)} %reshape.138, f32[16,16,64]{2,1,0:T(8,128)S(1)} %get-tuple-element.6, f32[16,16,64]{2,1,0:T(8,128)S(1)} %bitcast.81, f32[16,16,64]{2,1,0:T(8,128)S(1)} %mul.210), kind=kLoop, calls=%fused_computation.1 | loop fusion | flops 5242880 | bytes 8716288 | tf_op jit(solution)/shard_map/add | solution.py:117
  232.4 6.6 %fusion.81 = f32[16,16,1,64]{3,2,1,0:T(1,128)S(1)} fusion(f32[16,16,64,64]{3,2,1,0:T(8,128)S(1)} %multiply_add_fusion, bf16[16,16,64,1]{2,3,1,0:T(2,128)(2,1)S(1)} %reshape.149), kind=kOutput, calls=%fused_computation.97 | convolution fusion | flops 12582912 | bytes 4292608 | tf_op jit(solution)/shard_map/bhvk,bhk->bhv/dot_general | solution.py:121
  240.0 16.9 %all-gather.8.cloned.1.call-done = bf16[1024,2048]{0,1:T(8,128)(2,1)} async-done(((bf16[1024,128]{0,1:T(8,128)(2,1)}), bf16[1024,2048]{0,1:T(8,128)(2,1)}) %all-gather.8.cloned.1.call-update) | async-done | bytes 4194320 | tf_op jit(solution)/shard_map/all_gather | solution.py:51
  257.0 3.4 convolution_convert_fusion
  260.4 13.1 %all_to_all.72 = bf16[2,16,2048]{2,1,0:T(8,128)(2,1)S(1)} all-to-all(bf16[2,16,2048]{2,1,0:T(8,128)(2,1)S(1)} %broadcast_in_dim.8), channel_id=1, replica_groups=mesh['grp'=2,'ep_0'=16,'ep_1'=4,'tp'=2] {'tp'}, dimensions={0} | all-to-all | bytes 262144 | tf_op jit(solution)/shard_map/all_to_all | solution.py:41
  274.8 129.9 %all-gather.10.cloned.1.call-done = bf16[1024,2050]{1,0:T(8,128)(2,1)} async-done(((bf16[16,2050]{1,0:T(8,128)(2,1)}), bf16[1024,2050]{1,0:T(8,128)(2,1)}) %all-gather.10.cloned.1.call-update) | async-done | bytes 4198416 | tf_op jit(solution)/shard_map/all_gather | solution.py:61
  404.7 3.7 fusion.31
  410.5 3.7 fusion.35
  414.4 1.4 fusion.40
  418.6 10.4 %all-to-all-start.2 = ((s32[64,16,2]{1,2,0:T(2,128)}), s32[64,16,2]{1,2,0:T(2,128)S(1)}, u32[]{:S(2)}, u32[]{:S(2)}) async-start(s32[64,16,2]{1,2,0:T(2,128)} %stack.18), calls=%async_computation.2 | async-start | bytes 131072 | tf_op jit(solution)/shard_map/all_to_all | solution.py:21
  430.8 10.9 %all-to-all-done.2 = s32[64,16,2]{1,2,0:T(2,128)S(1)} async-done(((s32[64,16,2]{1,2,0:T(2,128)}), s32[64,16,2]{1,2,0:T(2,128)S(1)}, u32[]{:S(2)}, u32[]{:S(2)}) %all-to-all-start.2) | async-done | bytes 8224 | tf_op jit(solution)/shard_map/all_to_all | solution.py:21
  441.7 15.2 %all-to-all-start.3 = ((bf16[224,2,1024]{2,0,1:T(8,128)(2,1)}), bf16[224,2,1024]{2,0,1:T(8,128)(2,1)S(1)}, u32[]{:S(2)}, u32[]{:S(2)}) async-start(bf16[224,2,1024]{2,0,1:T(8,128)(2,1)} %bitcast.74), calls=%async_computation.3 | async-start | bytes 1835008 | tf_op jit(solution)/shard_map/all_to_all | solution.py:247
  457.4 3.4 fusion.27
  460.8 1.5 reshape.139
  463.1 1.4 reshape.134
  465.8 1.5 reshape.135
  467.6 3.7 all-to-all-start.4
  471.3 4.4 fusion.58
  475.7 4.4 fusion.8
  480.1 6.6 %all-to-all-start.5 = ((bf16[64,16,1024]{2,1,0:T(8,128)(2,1)}), bf16[64,16,1024]{2,1,0:T(8,128)(2,1)S(1)}, u32[]{:S(2)}, u32[]{:S(2)}) async-start(bf16[64,16,1024]{2,1,0:T(8,128)(2,1)} %bitcast.19), calls=%async_computation.5 | async-start | bytes 4194304 | tf_op jit(solution)/shard_map/all_to_all | solution.py:88
  486.7 96.3 %all-to-all-done.5 = bf16[64,16,1024]{2,1,0:T(8,128)(2,1)S(1)} async-done(((bf16[64,16,1024]{2,1,0:T(8,128)(2,1)}), bf16[64,16,1024]{2,1,0:T(8,128)(2,1)S(1)}, u32[]{:S(2)}, u32[]{:S(2)}) %all-to-all-start.5) | async-done | bytes 2097184 | tf_op jit(solution)/shard_map/all_to_all | solution.py:88
  583.3 6.9 %all_to_all.73 = f32[2,8,1024]{2,1,0:T(8,128)S(1)} all-to-all(f32[2,8,1024]{2,1,0:T(8,128)S(1)} %bitcast.83), channel_id=1, replica_groups=mesh['grp'=2,'ep_0'=16,'ep_1'=4,'tp'=2] {'tp'}, dimensions={0} | all-to-all | bytes 131072 | tf_op jit(solution)/shard_map/all_to_all | solution.py:257
  (100 shorter events, 17.3 us)
Async XLA Ops:
  7.2 403.3 %copy-start = (bf16[2048,224]{0,1:T(8,128)(2,1)S(1)}, bf16[2048,224]{0,1:T(8,128)(2,1)}, u32[]{:S(2)}) copy-start(bf16[2048,224]{0,1:T(8,128)(2,1)} %param.43) | copy-start | bytes 2752516
  7.2 183.1 %all-gather.6.cloned.1.call-start = ((), (), s32[]{:S(2)}) async-start(), calls=%async_computation.7 | async-start | bytes 12779520 | tf_op jit(solution)/shard_map/all_gather | solution.py:29
  9.0 248.0 %all-gather.8.cloned.1.call-start = ((), (), s32[]{:S(2)}) async-start(), calls=%async_computation.8 | async-start | bytes 4456448 | tf_op jit(solution)/shard_map/all_gather | solution.py:51
  22.0 382.7 %all-gather.10.cloned.1.call-start = ((), (), s32[]{:S(2)}) async-start(), calls=%async_computation.9 | async-start | bytes 4526080 | tf_op jit(solution)/shard_map/all_gather | solution.py:61
  232.4 6.6 %copy-start.2 = (f32[16,16,64,64]{3,2,1,0:T(8,128)}, f32[16,16,64,64]{3,2,1,0:T(8,128)S(1)}, u32[]{:S(2)}) copy-start(f32[16,16,64,64]{3,2,1,0:T(8,128)S(1)} %multiply_add_fusion) | copy-start | bytes 12582916
  232.4 7.0 %copy-start.7 = (f32[16,64]{1,0:T(8,128)S(1)}, f32[16,64]{1,0:T(8,128)}, u32[]{:S(2)}) copy-start(f32[16,64]{1,0:T(8,128)} %param.42) | copy-start | bytes 12292
  239.0 34.5 %copy-start.4 = (bf16[16,2048]{1,0:T(8,128)(2,1)S(1)}, bf16[16,2048]{1,0:T(8,128)(2,1)}, u32[]{:S(2)}) copy-start(bf16[16,2048]{1,0:T(8,128)(2,1)} %param.25) | copy-start | bytes 196612
  239.0 34.7 %copy-start.8 = (f32[2048]{0:T(1024)S(1)}, f32[2048]{0:T(1024)}, u32[]{:S(2)}) copy-start(f32[2048]{0:T(1024)} %param.30) | copy-start | bytes 24580
  239.0 165.7 %copy-start.12 = (bf16[2048,44]{0,1:T(8,128)(2,1)S(1)}, bf16[2048,44]{0,1:T(8,128)(2,1)}, u32[]{:S(2)}) copy-start(bf16[2048,44]{0,1:T(8,128)(2,1)} %param.46) | copy-start | bytes 540676
  274.5 134.0 %copy-start.13 = (bf16[2048,44]{0,1:T(8,128)(2,1)S(1)}, bf16[2048,44]{0,1:T(8,128)(2,1)}, u32[]{:S(2)}) copy-start(bf16[2048,44]{0,1:T(8,128)(2,1)} %param.47) | copy-start | bytes 540676
  274.5 186.3 %all-gather.12.cloned.1.call-start = ((), (), s32[]{:S(2)}) async-start(), calls=%async_computation.10 | async-start | bytes 1646592 | tf_op jit(solution)/shard_map/all_gather | solution.py:72
  404.7 3.7 copy-start.3
  410.0 4.3 slice-start
  410.5 3.8 slice-start.1
  410.5 3.8 copy-start.11
  414.3 3.6 copy-start.10
  414.3 14.7 %copy-start.9 = (bf16[2048]{0:T(1024)(128)(2,1)S(1)}, bf16[2048]{0:T(1024)(128)(2,1)}, u32[]{:S(2)}) copy-start(bf16[2048]{0:T(1024)(128)(2,1)} %param.49) | copy-start | bytes 12292
  414.3 14.7 %copy-start.6 = (bf16[44,2048]{1,0:T(8,128)(2,1)S(1)}, bf16[44,2048]{1,0:T(8,128)(2,1)}, u32[]{:S(2)}) copy-start(bf16[44,2048]{1,0:T(8,128)(2,1)} %param.48) | copy-start | bytes 540676
  415.8 14.0 %copy-start.5 = (bf16[224,2048]{1,0:T(8,128)(2,1)S(1)}, bf16[224,2048]{1,0:T(8,128)(2,1)}, u32[]{:S(2)}) copy-start(bf16[224,2048]{1,0:T(8,128)(2,1)} %param.45) | copy-start | bytes 2752516
  416.0 41.2 %slice-start.2 = ((bf16[1024,2050]{1,0:T(8,128)(2,1)}), bf16[1024,2]{1,0:T(8,128)(2,1)S(1)}, s32[]{:S(2)}) async-start(bf16[1024,2050]{1,0:T(8,128)(2,1)} %all-gather.10.cloned.1.call-done), calls=%async_computation.13 | async-start | bytes 524288 | tf_op jit(solution)/shard_map/split | solution.py:61
  418.6 23.1 %all-to-all-start.2 = ((s32[64,16,2]{1,2,0:T(2,128)}), s32[64,16,2]{1,2,0:T(2,128)S(1)}, u32[]{:S(2)}, u32[]{:S(2)}) async-start(s32[64,16,2]{1,2,0:T(2,128)} %stack.18), calls=%async_computation.2 | async-start | bytes 131072 | tf_op jit(solution)/shard_map/all_to_all | solution.py:21
  441.7 25.9 %all-to-all-start.3 = ((bf16[224,2,1024]{2,0,1:T(8,128)(2,1)}), bf16[224,2,1024]{2,0,1:T(8,128)(2,1)S(1)}, u32[]{:S(2)}, u32[]{:S(2)}) async-start(bf16[224,2,1024]{2,0,1:T(8,128)(2,1)} %bitcast.74), calls=%async_computation.3 | async-start | bytes 1835008 | tf_op jit(solution)/shard_map/all_to_all | solution.py:247
  467.6 8.2 %all-to-all-start.4 = ((bf16[44,2,1024]{2,0,1:T(8,128)(2,1)}), bf16[44,2,1024]{2,0,1:T(8,128)(2,1)S(1)}, u32[]{:S(2)}, u32[]{:S(2)}) async-start(bf16[44,2,1024]{2,0,1:T(8,128)(2,1)} %copy.92), calls=%async_computation.4 | async-start | bytes 393216 | tf_op jit(solution)/shard_map/all_to_all | solution.py:248
  475.7 115.1 %copy-start.1 = (bf16[2048,224]{0,1:T(8,128)(2,1)S(1)}, bf16[2048,224]{0,1:T(8,128)(2,1)}, u32[]{:S(2)}) copy-start(bf16[2048,224]{0,1:T(8,128)(2,1)} %param.43) | copy-start | bytes 2752516
  480.1 102.9 %all-to-all-start.5 = ((bf16[64,16,1024]{2,1,0:T(8,128)(2,1)}), bf16[64,16,1024]{2,1,0:T(8,128)(2,1)S(1)}, u32[]{:S(2)}, u32[]{:S(2)}) async-start(bf16[64,16,1024]{2,1,0:T(8,128)(2,1)} %bitcast.19), calls=%async_computation.5 | async-start | bytes 4194304 | tf_op jit(solution)/shard_map/all_to_all | solution.py:88
Sparse Core Ops, SparseCore 0:
  11.0 179.2 all-gather.5
  192.1 64.8 all-gather.7
  274.6 130.0 all-gather.9
  418.0 23.4 all-gather.11
